TPU v7x, 32 devices: a whole 2x2x4 slice. The times are simulated.
32 devices in a mesh: ep: 16 (over z, y, x), tp: 2 (over core).
Axes of the slice: x: 2, y: 2, z: 4, core: 2. Of those that a mesh axis runs over, the one named last changes fastest.
Arguments:
- tokens: bfloat16 [112, 2304], P('ep'), may hold values from -6 to 6
- attn_gain: bfloat16 [2304], replicated, may hold values from 0.099609375 to 1.8984375
- query_weight: bfloat16 [2304, 2048], P(None, 'tp'), may hold values from -0.125 to 0.125
- key_weight: bfloat16 [2304, 2048], P(None, 'tp'), may hold values from -0.125 to 0.125
- value_weight: bfloat16 [2304, 2048], P(None, 'tp'), may hold values from -0.125 to 0.125
- out_weight: bfloat16 [2304, 2048], P(None, 'tp'), may hold values from -0.125 to 0.125
- lambdas: float32 [16], P('tp'), may hold values from 0.3 to 0.8
- head_gain: bfloat16 [128], replicated, may hold values from 0.099609375 to 1.8984375
- cache_keys: bfloat16 [112, 1024, 16, 128], P('ep', None, 'tp'), may hold values from -1500 to 1500
- cache_values: bfloat16 [112, 1024, 16, 128], P('ep', None, 'tp'), may hold values from -6 to 6
- lengths: int32 [112], P('ep'), may hold values from 2 to 1024, as said below
- moe_gain: bfloat16 [2304], replicated, may hold values from 0.099609375 to 1.8984375
- gate_weight: bfloat16 [16, 2304, 1024], P('ep', None, 'tp'), may hold values from -0.125 to 0.125
- up_weight: bfloat16 [16, 2304, 1024], P('ep', None, 'tp'), may hold values from -0.125 to 0.125
- down_weight: bfloat16 [16, 1024, 2304], P('ep', 'tp'), may hold values from -0.1875 to 0.1875
- shared_gate: bfloat16 [2304, 1024], P(None, 'tp'), may hold values from -0.125 to 0.125
- shared_up: bfloat16 [2304, 1024], P(None, 'tp'), may hold values from -0.125 to 0.125
- shared_down: bfloat16 [1024, 2304], P('tp'), may hold values from -0.1875 to 0.1875
- expert_ids: int32 [112, 6], P('ep'), may hold values from 0 to 15, all different within a row; in each aligned block of 7 rows (0 to 6, 7 to 13, ...) at most 5 rows name the same one
- expert_weights: float32 [112, 6], P('ep'), may hold values from 0.2 to 1
Outputs:
- result: bfloat16 [112, 2304], P('ep', 'tp')
Inputs may be any that keep to these rules, and one draw needn't show every extreme that they name: `expert_ids`: each row names 6 different experts. Among the rows of one device (aligned blocks of 7 rows) no expert is named by more than 5 rows, a bound that some block reaches. `lengths`: some sequence has 1024 cached positions.
All inputs are finite; a program needn't handle non-finite values.
Results may differ from a plain program's by a relative error of at most 0.02.
Values may be sent and summed in bfloat16 or wider, within the bound.
No kernel may reach another device: no remote copies, remote signals or barrier semaphores. Data moves between devices by JAX's collectives and lax.ppermute only.
A program may use at most 128 MiB of HBM per device.

v0:
```python
import jax
import jax.numpy as jnp
from jax import lax
from jax.sharding import PartitionSpec as P

epsilon = 1e-06


def rms_scale(values, gain):
    wide = values.astype(jnp.float32)
    return (
        wide
        * lax.rsqrt(jnp.mean(wide * wide, axis=-1, keepdims=True) + epsilon)
        * gain.astype(jnp.float32)
    )


def shards(
    tokens,
    attn_gain,
    query_weight,
    key_weight,
    value_weight,
    out_weight,
    lambdas,
    head_gain,
    cache_keys,
    cache_values,
    lengths,
    moe_gain,
    gate_weight,
    up_weight,
    down_weight,
    shared_gate,
    shared_up,
    shared_down,
    expert_ids,
    expert_weights,
):
    seq_dev, model_width = tokens.shape
    local_heads = lambdas.shape[0]
    head_dim = cache_keys.shape[-1] // 2
    cache_len = cache_keys.shape[1]
    normed = rms_scale(tokens, attn_gain).astype(jnp.bfloat16)
    query_rows = jnp.dot(normed, query_weight, preferred_element_type=jnp.float32).astype(
        jnp.bfloat16
    )
    key_new = jnp.dot(normed, key_weight, preferred_element_type=jnp.float32).astype(jnp.bfloat16)
    value_new = jnp.dot(normed, value_weight, preferred_element_type=jnp.float32).astype(
        jnp.bfloat16
    )
    score_scale = head_dim ** (-0.5)
    queries = query_rows.reshape(seq_dev, local_heads, 2, head_dim)
    new_keys = key_new.reshape(seq_dev, local_heads, 2, head_dim)
    new_values = value_new.reshape(seq_dev, local_heads, 2 * head_dim)
    past_keys = cache_keys.reshape(seq_dev, cache_len, local_heads, 2, head_dim)
    scores = (
        jnp.einsum("shmd,sjhmd->shmj", queries, past_keys, preferred_element_type=jnp.float32)
        * score_scale
    )
    own_score = (
        jnp.sum(queries.astype(jnp.float32) * new_keys.astype(jnp.float32), axis=-1) * score_scale
    )
    live_mask = (jnp.arange(cache_len, dtype=jnp.int32)[None, :] < lengths[:, None])[
        :, None, None, :
    ]
    peak_score = jnp.maximum(jnp.max(jnp.where(live_mask, scores, -jnp.inf), axis=-1), own_score)
    exp_terms = jnp.where(live_mask, jnp.exp(scores - peak_score[..., None]), 0.0)
    own_term = jnp.exp(own_score - peak_score)
    denom_sum = jnp.sum(exp_terms, axis=-1) + own_term
    map_probs = exp_terms / denom_sum[..., None]
    own_prob = own_term / denom_sum
    lambda_row = lambdas[None, :]
    mixture = (map_probs[:, :, 0] - lambda_row[..., None] * map_probs[:, :, 1]).astype(jnp.bfloat16)
    own_mixture = (own_prob[:, :, 0] - lambda_row * own_prob[:, :, 1]).astype(jnp.bfloat16)
    head_out = jnp.einsum(
        "shj,sjhv->shv", mixture, cache_values, preferred_element_type=jnp.float32
    )
    head_out = head_out + own_mixture.astype(jnp.float32)[..., None] * new_values.astype(
        jnp.float32
    )
    head_normed = (
        rms_scale(head_out, head_gain)
        .astype(jnp.bfloat16)
        .reshape(seq_dev, local_heads * 2 * head_dim)
    )
    attn_part = lax.dot_general(
        head_normed, out_weight, (((1,), (1,)), ((), ())), preferred_element_type=jnp.float32
    )
    attn_total = lax.psum(attn_part.astype(jnp.bfloat16), "tp").astype(jnp.float32)
    mixed_rows = (tokens.astype(jnp.float32) + attn_total).astype(jnp.bfloat16)
    moe_normed = rms_scale(mixed_rows, moe_gain).astype(jnp.bfloat16)
    shared_gate_out = jnp.dot(moe_normed, shared_gate, preferred_element_type=jnp.float32)
    shared_up_out = jnp.dot(moe_normed, shared_up, preferred_element_type=jnp.float32)
    shared_hidden = (jax.nn.silu(shared_gate_out) * shared_up_out).astype(jnp.bfloat16)
    shared_part = jnp.dot(shared_hidden, shared_down, preferred_element_type=jnp.float32)
    experts = lax.axis_size("ep")
    top_count = expert_ids.shape[1]
    capacity = min(seq_dev, max(2, 2 * seq_dev * top_count // experts))
    slot_count = seq_dev * top_count
    slot_ids = expert_ids.reshape(slot_count)
    expert_hits = (slot_ids[:, None] == jnp.arange(experts, dtype=jnp.int32)[None, :]).astype(
        jnp.int32
    )
    slot_rank = jnp.sum((jnp.cumsum(expert_hits, axis=0) - expert_hits) * expert_hits, axis=1)
    slot_place = slot_ids * capacity + slot_rank
    placed = (
        slot_place[:, None] == jnp.arange(experts * capacity, dtype=jnp.int32)[None, :]
    ).astype(jnp.bfloat16)
    slot_token = jnp.arange(slot_count, dtype=jnp.int32) // top_count
    token_pick = (slot_token[:, None] == jnp.arange(seq_dev, dtype=jnp.int32)[None, :]).astype(
        jnp.bfloat16
    )
    dispatch = lax.dot_general(
        placed, token_pick, (((0,), (0,)), ((), ())), preferred_element_type=jnp.float32
    ).astype(jnp.bfloat16)
    col_count = model_width // lax.axis_size("tp")
    own_start = lax.axis_index("tp") * col_count
    own_normed = lax.dynamic_slice_in_dim(moe_normed, own_start, col_count, 1)
    send_slice = jnp.dot(dispatch, own_normed, preferred_element_type=jnp.float32).astype(
        jnp.bfloat16
    )
    arrived = lax.all_to_all(send_slice, "ep", split_axis=0, concat_axis=0, tiled=True)
    received = lax.all_gather(arrived, "tp", axis=1, tiled=True)
    gate_out = jnp.dot(received, gate_weight[0], preferred_element_type=jnp.float32)
    up_out = jnp.dot(received, up_weight[0], preferred_element_type=jnp.float32)
    expert_hidden = (jax.nn.silu(gate_out) * up_out).astype(jnp.bfloat16)
    expert_part = jnp.dot(expert_hidden, down_weight[0], preferred_element_type=jnp.float32)
    expert_sum, shared_out = (
        lax.psum_scatter(
            expert_part.astype(jnp.bfloat16), "tp", scatter_dimension=1, tiled=True
        ).astype(jnp.float32),
        lax.psum_scatter(
            shared_part.astype(jnp.bfloat16), "tp", scatter_dimension=1, tiled=True
        ).astype(jnp.float32),
    )
    returned = lax.all_to_all(
        expert_sum.astype(jnp.bfloat16), "ep", split_axis=0, concat_axis=0, tiled=True
    )
    slot_values = jnp.dot(placed, returned, preferred_element_type=jnp.float32).reshape(
        seq_dev, top_count, col_count
    )
    routed = jnp.sum(expert_weights[:, :, None] * slot_values, axis=1)
    own_cols = lax.dynamic_slice_in_dim(mixed_rows, own_start, col_count, 1)
    return (own_cols.astype(jnp.float32) + routed + shared_out).astype(jnp.bfloat16)


def solution(mesh):
    in_specs = (
        P("ep", None),
        P(),
        P(None, "tp"),
        P(None, "tp"),
        P(None, "tp"),
        P(None, "tp"),
        P("tp"),
        P(),
        P("ep", None, "tp", None),
        P("ep", None, "tp", None),
        P("ep"),
        P(),
        P("ep", None, "tp"),
        P("ep", None, "tp"),
        P("ep", "tp", None),
        P(None, "tp"),
        P(None, "tp"),
        P("tp", None),
        P("ep", None),
        P("ep", None),
    )
    out_specs = P("ep", "tp")
    return jax.shard_map(shards, mesh=mesh, in_specs=in_specs, out_specs=out_specs, check_vma=False)
```

profile of v0, /device:TPU:0, one launch (start us, length us, event | category | flops | bytes accessed | tf_op | source)
XLA Modules:
  0.0 123.7 jit_solution(13733338271488698938)
XLA Ops:
  6.5 0.8 convert_element_type.102
  7.4 0.9 fusion.36
  8.3 3.1 %convolution_convert_fusion.6 = bf16[7,1024]{1,0:T(8,128)(2,1)S(1)} fusion(bf16[2304,1024]{1,0:T(8,128)(2,1)} %param.22, bf16[7,2304]{1,0:T(8,128)(2,1)} %param.20, f32[2304]{0:T(1024)S(1)} %convert_element_type.102, f32[7]{0:T(128)S(1)} %add_rsqrt_fusion.2), kind=kOutput, calls=%fused_computation.20 | convolution fusion | flops 33101824 | bytes 4774428 | tf_op jit(solution)/shard_map/dot_general | solution.py:45
  11.6 20.6 %copy.40 = bf16[7,1024,8,128]{1,3,2,0:T(8,128)(2,1)} copy(bf16[7,1024,8,128]{3,2,1,0:T(8,128)(2,1)} %param.28) | data formatting | bytes 29360128 | tf_op args[8]
  32.3 3.1 %fusion.18 = f32[7,1024]{1,0:T(8,128)S(1)} fusion(bf16[2304,1024]{1,0:T(8,128)(2,1)} %param.23, bf16[7,2304]{1,0:T(8,128)(2,1)S(1)} %copy-done.1, f32[2304]{0:T(1024)S(1)} %convert_element_type.102, f32[7]{0:T(128)S(1)} %add_rsqrt_fusion.2), kind=kOutput, calls=%fused_computation.19 | convolution fusion | flops 33108992 | bytes 4788764 | tf_op jit(solution)/shard_map/dot_general | solution.py:48
  35.8 7.3 %fusion.69 = f32[7,8,2,1,1024]{4,3,2,1,0:T(1,128)S(1)} fusion(bf16[7,8,2,64,1]{3,4,2,1,0:T(2,128)(2,1)S(1)} %reshape.146, bf16[7,1024,8,2,64]{1,4,3,2,0:T(8,128)(2,1)} %bitcast.87), kind=kOutput, calls=%fused_computation.101 | convolution fusion | flops 14680064 | bytes 15153152 | tf_op jit(solution)/shard_map/shmd,sjhmd->shmj/dot_general | solution.py:58
  44.2 0.8 fusion.17
  44.9 7.6 %fusion = f32[7,8,1,128]{3,2,1,0:T(1,128)S(1)} fusion(bf16[7,1024,8,128]{3,2,1,0:T(8,128)(2,1)} %param.29, bf16[7,8,1024,1]{2,1,0,3:T(8,128)(2,1)S(1)} %fusion.31), kind=kOutput, calls=%fused_computation | convolution fusion | flops 14680064 | bytes 14823424 | tf_op jit(solution)/shard_map/shj,sjhv->shv/dot_general | solution.py:76
  52.9 1.3 %convolution_convert_fusion.2 = bf16[7,2304]{1,0:T(8,128)(2,1)S(1)} fusion(bf16[2304,1024]{1,0:T(8,128)(2,1)S(1)} %bitcast.91, bf16[1,7,8,128]{3,2,1,0:T(8,128)(2,1)S(1)} %fusion.52), kind=kOutput, calls=%fused_computation.4 | convolution fusion | flops 33046272 | bytes 4765184 | tf_op jit(solution)/shard_map/dot_general | solution.py:87
  54.2 3.8 %psum.7 = bf16[7,2304]{1,0:T(8,128)(2,1)S(1)} all-reduce(bf16[7,2304]{1,0:T(8,128)(2,1)S(1)} %convolution_convert_fusion.2), channel_id=1, replica_groups=mesh['ep'=16,'tp'=2] {'tp'}, use_global_device_ids=true, to_apply=%region_5.6 | all-reduce | flops 16128 | bytes 64512 | tf_op jit(solution)/shard_map/psum | solution.py:90
  59.2 19.0 %all_to_all.24 = bf16[16,5,1152]{2,1,0:T(8,128)(2,1)S(1)} all-to-all(bf16[16,5,1152]{2,1,0:T(8,128)(2,1)S(1)} %all_to_all.16), channel_id=1, replica_groups=mesh['ep'=16,'tp'=2] {'ep'}, dimensions={0} | all-to-all | bytes 368640 | tf_op jit(solution)/shard_map/all_to_all | solution.py:123
  78.4 2.1 %all_gather.3 = bf16[80,2304]{1,0:T(8,128)(2,1)S(1)} all-gather(bf16[80,1152]{1,0:T(8,128)(2,1)S(1)} %all_to_all.18), channel_id=1, replica_groups=mesh['ep'=16,'tp'=2] {'tp'}, dimensions={1}, use_global_device_ids=true | all-gather | bytes 552960 | tf_op jit(solution)/shard_map/all_gather | solution.py:124
  80.4 2.2 %fusion.5 = f32[80,512]{1,0:T(8,128)S(1)} fusion(bf16[80,2304]{1,0:T(8,128)(2,1)S(1)} %all_gather.3, bf16[1,2304,512]{2,1,0:T(8,128)(2,1)} %param.32), kind=kOutput, calls=%fused_computation.8 | convolution fusion | flops 188743680 | bytes 2891776 | tf_op jit(solution)/shard_map/dot_general | solution.py:125
  82.6 2.6 %convolution_convert_fusion = bf16[80,2304]{1,0:T(8,128)(2,1)S(1)} fusion(bf16[1,512,2304]{2,1,0:T(8,128)(2,1)S(1)} %copy-done, bf16[80,2304]{1,0:T(8,128)(2,1)S(1)} %all_gather.3, bf16[1,2304,512]{2,1,0:T(8,128)(2,1)} %param.33, f32[80,512]{1,0:T(8,128)S(1)} %fusion.5), kind=kOutput, calls=%fused_computation.2 | convolution fusion | flops 377917440 | bytes 5619712 | tf_op jit(solution)/shard_map/dot_general | solution.py:128
  85.2 1.1 copy.50
  86.3 2.1 %fusion.70 = f32[7,512]{1,0:T(8,128)S(1)} fusion(bf16[7,2304]{1,0:T(8,128)(2,1)S(1)} %fusion.35, bf16[2304,512]{1,0:T(8,128)(2,1)} %param.35), kind=kOutput, calls=%fused_computation.102 | convolution fusion | flops 16515072 | bytes 2405888 | tf_op jit(solution)/shard_map/dot_general | solution.py:93
  88.4 3.9 %reduce-scatter.7.cloned.1.call-done = bf16[1152,80]{1,0:T(8,128)(2,1)} async-done(((bf16[2304,80]{1,0:T(8,128)(2,1)}), bf16[1152,80]{1,0:T(8,128)(2,1)}) %reduce-scatter.7.cloned.1.call-update) | async-done | bytes 184336
  92.3 1.1 copy.51
  93.4 0.8 all_to_all.19
  94.2 6.7 %all-to-all-start.1 = ((bf16[16,5,1152]{2,1,0:T(8,128)(2,1)}), bf16[16,5,1152]{2,1,0:T(8,128)(2,1)S(1)}, u32[]{:S(2)}, u32[]{:S(2)}) async-start(bf16[16,5,1152]{2,1,0:T(8,128)(2,1)} %all_to_all.19), calls=%async_computation.1 | async-start | bytes 589824 | tf_op jit(solution)/shard_map/all_to_all | solution.py:137
  101.0 3.2 %convolution_convert_fusion.1 = bf16[7,2304]{1,0:T(8,128)(2,1)S(1)} fusion(bf16[512,2304]{1,0:T(8,128)(2,1)} %param.37, bf16[7,2304]{1,0:T(8,128)(2,1)S(1)} %fusion.35, bf16[2304,512]{1,0:T(8,128)(2,1)} %param.36, f32[7,512]{1,0:T(8,128)S(1)} %fusion.70), kind=kOutput, calls=%fused_computation.3 | convolution fusion | flops 33067776 | bytes 4797440 | tf_op jit(solution)/shard_map/dot_general | solution.py:96
  104.2 1.1 copy.52
  105.6 9.2 %reduce-scatter.9.cloned.1.call-done = bf16[1152,7]{1,0:T(8,128)(2,1)} async-done(((bf16[2304,7]{1,0:T(8,128)(2,1)}), bf16[1152,7]{1,0:T(8,128)(2,1)}) %reduce-scatter.9.cloned.1.call-update) | async-done | bytes 16144
  114.8 1.1 copy.53
  (69 shorter events, 4.5 us)
Async XLA Ops:
  6.5 76.1 %copy-start = (bf16[1,512,2304]{2,1,0:T(8,128)(2,1)S(1)}, bf16[1,512,2304]{2,1,0:T(8,128)(2,1)}, u32[]{:S(2)}) copy-start(bf16[1,512,2304]{2,1,0:T(8,128)(2,1)} %param.34) | copy-start | bytes 7077892
  6.5 85.7 %reduce-scatter.7.cloned.1.call-start = ((), (), s32[]{:S(2)}) async-start(), calls=%async_computation.4 | async-start | bytes 884736
  11.6 20.6 %copy-start.6 = (s32[7]{0:T(128)S(1)}, s32[7]{0:T(128)}, u32[]{:S(2)}) copy-start(s32[7]{0:T(128)} %param.30) | copy-start | bytes 88
  11.6 20.7 %copy-start.1 = (bf16[7,2304]{1,0:T(8,128)(2,1)S(1)}, bf16[7,2304]{1,0:T(8,128)(2,1)}, u32[]{:S(2)}) copy-start(bf16[7,2304]{1,0:T(8,128)(2,1)} %param.20) | copy-start | bytes 96772
  32.3 11.9 %slice-start = ((s8[4718592]{0:T(1024)(128)(4,1)}), s8[524288]{0:T(1024)(128)(4,1)S(1)}, s32[]{:S(2)}) async-start(s8[4718592]{0:T(1024)(128)(4,1)} %bitcast.88), calls=%async_computation.6 | async-start | bytes 1048576
  35.8 8.2 %copy-start.5 = (f32[8]{0:T(128)S(1)}, f32[8]{0:T(128)}, u32[]{:S(2)}) copy-start(f32[8]{0:T(128)} %param.26) | copy-start | bytes 100
  35.8 8.3 %slice-start.1 = ((s8[4718592]{0:T(1024)(128)(4,1)}), s8[4194304]{0:T(1024)(128)(4,1)S(1)}, s32[]{:S(2)}) async-start(s8[4718592]{0:T(1024)(128)(4,1)} %bitcast.88), calls=%async_computation.7 | async-start | bytes 8388608
  44.2 8.7 %slice-start.2 = ((s8[4718592]{0:T(1024)(128)(4,1)}), s8[4194304]{0:T(1024)(128)(4,1)S(1)}, s32[]{:S(2)}) async-start(s8[4718592]{0:T(1024)(128)(4,1)} %bitcast.90), calls=%async_computation.8 | async-start | bytes 8388608
  44.9 7.8 %copy-start.7 = (bf16[128]{0:T(256)(128)(2,1)S(1)}, bf16[128]{0:T(256)(128)(2,1)}, u32[]{:S(2)}) copy-start(bf16[128]{0:T(256)(128)(2,1)} %param.27) | copy-start | bytes 772
  44.9 7.9 %slice-start.3 = ((s8[4718592]{0:T(1024)(128)(4,1)}), s8[524288]{0:T(1024)(128)(4,1)S(1)}, s32[]{:S(2)}) async-start(s8[4718592]{0:T(1024)(128)(4,1)} %bitcast.90), calls=%async_computation.9 | async-start | bytes 1048576
  52.6 5.6 %copy-start.3 = (bf16[2304]{0:T(1024)(128)(2,1)S(1)}, bf16[2304]{0:T(1024)(128)(2,1)}, u32[]{:S(2)}) copy-start(bf16[2304]{0:T(1024)(128)(2,1)} %param.31) | copy-start | bytes 13828
  52.6 5.6 %copy-start.2 = (s32[7,6]{1,0:T(8,128)S(1)}, s32[7,6]{1,0:T(8,128)}, u32[]{:S(2)}) copy-start(s32[7,6]{1,0:T(8,128)} %param.38) | copy-start | bytes 508
  86.3 19.2 %copy-start.4 = (f32[7,6]{1,0:T(8,128)S(1)}, f32[7,6]{1,0:T(8,128)}, u32[]{:S(2)}) copy-start(f32[7,6]{1,0:T(8,128)} %param.39) | copy-start | bytes 508
  94.2 21.7 %all-to-all-start.1 = ((bf16[16,5,1152]{2,1,0:T(8,128)(2,1)}), bf16[16,5,1152]{2,1,0:T(8,128)(2,1)S(1)}, u32[]{:S(2)}, u32[]{:S(2)}) async-start(bf16[16,5,1152]{2,1,0:T(8,128)(2,1)} %all_to_all.19), calls=%async_computation.1 | async-start | bytes 589824 | tf_op jit(solution)/shard_map/all_to_all | solution.py:137
  100.9 13.8 %reduce-scatter.9.cloned.1.call-start = ((), (), s32[]{:S(2)}) async-start(), calls=%async_computation.5 | async-start | bytes 884736
Sparse Core Ops, SparseCore 0:
  86.4 5.7 reduce-scatter.6
  105.4 9.2 reduce-scatter.8
where the time goes:
time: 125 us; the launch traced here: 124 us
  matrix products  34.1 us (27%)
  local copies, waits for them, and re-layouts  26.8 us (21%)
  blocking collectives  24.9 us (20%)
  between operations  13.7 us (11%)
  waiting for transfers between devices  13.1 us (10%)
  starting transfers between devices  6.78 us (5%)
  other arithmetic  4.34 us (3%)
    unnamed x31, local copies, waits for them, and re-layouts  25.1 us
    all_to_all x1, blocking collectives, shards(): lax.all_to_all(send_slice, 'ep', split_axis=0, concat_axis=0, tiled=True)  19 us
    unnamed x4, waiting for transfers between devices  13.1 us
    dot_general x1, matrix products, shards(): jnp.einsum('shj,sjhv->shv', mixture, cache_values, preferred_element_type...  7.61 us
    dot_general x1, matrix products, shards(): jnp.einsum('shmd,sjhmd->shmj', queries, past_keys, preferred_element_type...  7.34 us
    all_to_all x1, starting transfers between devices, shards(): lax.all_to_all(expert_sum.astype(jnp.bfloat16), 'ep', split_axis=0, conca...  6.73 us
    psum x1, blocking collectives, shards(): lax.psum(attn_part.astype(jnp.bfloat16), 'tp').astype(jnp.float32)  3.78 us
    dot_general x1, matrix products, shards(): jnp.dot(shared_hidden, shared_down, preferred_element_type=jnp.float32)  3.2 us
  transfers between devices with their start and end apart: 3, of which 2 were waited for; matrix products, arithmetic and copies ran while one was open for 6% of the time, Pallas kernels for 0%

commit v1 on v0

--- a/solution.py
+++ b/solution.py
@@ -4,6 +4,12 @@
 from jax.sharding import PartitionSpec as P
 
 epsilon = 1e-06
+
+
+def lead_loops(tile_in):
+    arr_out = jax.lax.all_gather(tile_in, axis_name="tp")
+    w_next = jnp.sum(arr_out, axis=0)
+    return w_next
 
 
 def rms_scale(values, gain):
@@ -87,7 +93,7 @@
     attn_part = lax.dot_general(
         head_normed, out_weight, (((1,), (1,)), ((), ())), preferred_element_type=jnp.float32
     )
-    attn_total = lax.psum(attn_part.astype(jnp.bfloat16), "tp").astype(jnp.float32)
+    attn_total = lead_loops(attn_part.astype(jnp.bfloat16)).astype(jnp.float32)
     mixed_rows = (tokens.astype(jnp.float32) + attn_total).astype(jnp.bfloat16)
     moe_normed = rms_scale(mixed_rows, moe_gain).astype(jnp.bfloat16)
     shared_gate_out = jnp.dot(moe_normed, shared_gate, preferred_element_type=jnp.float32)

time: 125 us -> 123 us (0.984)
  blocking collectives: 24.9 us -> 23.1 us
    psum x1 -> x0, blocking collectives: 3.78 us -> none  [shards(): lax.psum(attn_part.astype(jnp.bfloat16), 'tp').astype(jnp.float32)]
    all_gather x0 -> x1, blocking collectives: none -> 2.01 us  [lead_loops(): arr_out = jax.lax.all_gather(tile_in, axis_name='tp')]
where the time goes in v1:
time: 123 us; the launch traced here: 122 us
  matrix products  34.1 us (28%)
  local copies, waits for them, and re-layouts  26.8 us (22%)
  blocking collectives  23.1 us (19%)
  between operations  13.7 us (11%)
  waiting for transfers between devices  13.1 us (11%)
  starting transfers between devices  6.78 us (6%)
  other arithmetic  4.36 us (4%)
    unnamed x31, local copies, waits for them, and re-layouts  25.1 us
    all_to_all x1, blocking collectives, shards(): lax.all_to_all(send_slice, 'ep', split_axis=0, concat_axis=0, tiled=True)  19 us
    unnamed x4, waiting for transfers between devices  13.1 us
    dot_general x1, matrix products, shards(): jnp.einsum('shj,sjhv->shv', mixture, cache_values, preferred_element_type...  7.61 us
    dot_general x1, matrix products, shards(): jnp.einsum('shmd,sjhmd->shmj', queries, past_keys, preferred_element_type...  7.34 us
    all_to_all x1, starting transfers between devices, shards(): lax.all_to_all(expert_sum.astype(jnp.bfloat16), 'ep', split_axis=0, conca...  6.74 us
    dot_general x1, matrix products, shards(): jnp.dot(shared_hidden, shared_down, preferred_element_type=jnp.float32)  3.2 us
    dot_general x1, matrix products, shards(): jnp.dot(normed, key_weight, preferred_element_type=jnp.float32)  3.15 us
  transfers between devices with their start and end apart: 3, of which 2 were waited for; matrix products, arithmetic and copies ran while one was open for 6% of the time, Pallas kernels for 0%

profile of v1, /device:TPU:0, one launch (start us, length us, event | category | flops | bytes accessed | tf_op | source)
XLA Modules:
  0.0 121.9 jit_solution(9992183582123899538)
XLA Ops:
  6.5 0.8 convert_element_type.104
  7.4 0.9 fusion.37
  8.3 3.1 %convolution_convert_fusion.6 = bf16[7,1024]{1,0:T(8,128)(2,1)S(1)} fusion(bf16[2304,1024]{1,0:T(8,128)(2,1)} %param.22, bf16[7,2304]{1,0:T(8,128)(2,1)} %param.20, f32[2304]{0:T(1024)S(1)} %convert_element_type.104, f32[7]{0:T(128)S(1)} %add_rsqrt_fusion.2), kind=kOutput, calls=%fused_computation.21 | convolution fusion | flops 33101824 | bytes 4774428 | tf_op jit(solution)/shard_map/dot_general | solution.py:51
  11.6 20.6 %copy.40 = bf16[7,1024,8,128]{1,3,2,0:T(8,128)(2,1)} copy(bf16[7,1024,8,128]{3,2,1,0:T(8,128)(2,1)} %param.28) | data formatting | bytes 29360128 | tf_op args[8]
  32.3 3.1 %fusion.19 = f32[7,1024]{1,0:T(8,128)S(1)} fusion(bf16[2304,1024]{1,0:T(8,128)(2,1)} %param.23, bf16[7,2304]{1,0:T(8,128)(2,1)S(1)} %copy-done.1, f32[2304]{0:T(1024)S(1)} %convert_element_type.104, f32[7]{0:T(128)S(1)} %add_rsqrt_fusion.2), kind=kOutput, calls=%fused_computation.20 | convolution fusion | flops 33108992 | bytes 4788764 | tf_op jit(solution)/shard_map/dot_general | solution.py:54
  35.8 7.3 %fusion.70 = f32[7,8,2,1,1024]{4,3,2,1,0:T(1,128)S(1)} fusion(bf16[7,8,2,64,1]{3,4,2,1,0:T(2,128)(2,1)S(1)} %reshape.150, bf16[7,1024,8,2,64]{1,4,3,2,0:T(8,128)(2,1)} %bitcast.89), kind=kOutput, calls=%fused_computation.102 | convolution fusion | flops 14680064 | bytes 15153152 | tf_op jit(solution)/shard_map/shmd,sjhmd->shmj/dot_general | solution.py:64
  44.2 0.8 fusion.18
  44.9 7.6 %fusion = f32[7,8,1,128]{3,2,1,0:T(1,128)S(1)} fusion(bf16[7,1024,8,128]{3,2,1,0:T(8,128)(2,1)} %param.29, bf16[7,8,1024,1]{2,1,0,3:T(8,128)(2,1)S(1)} %fusion.32), kind=kOutput, calls=%fused_computation | convolution fusion | flops 14680064 | bytes 14823424 | tf_op jit(solution)/shard_map/shj,sjhv->shv/dot_general | solution.py:82
  52.9 1.3 %fusion.2 = bf16[1,7,2304]{2,1,0:T(8,128)(2,1)S(1)} fusion(bf16[2304,1024]{1,0:T(8,128)(2,1)S(1)} %bitcast.93, bf16[1,7,8,128]{3,2,1,0:T(8,128)(2,1)S(1)} %fusion.53), kind=kOutput, calls=%fused_computation.5 | convolution fusion | flops 33046272 | bytes 4765184 | tf_op jit(solution)/shard_map/dot_general | solution.py:93
  54.2 2.0 %all-gather.1 = bf16[2,7,2304]{2,1,0:T(8,128)(2,1)S(1)} all-gather(bf16[1,7,2304]{2,1,0:T(8,128)(2,1)S(1)} %fusion.2), channel_id=2, replica_groups=mesh['ep'=16,'tp'=2] {'tp'}, dimensions={0}, use_global_device_ids=true | all-gather | bytes 96768 | tf_op jit(solution)/shard_map/all_gather | solution.py:10
  57.5 19.0 %all_to_all.24 = bf16[16,5,1152]{2,1,0:T(8,128)(2,1)S(1)} all-to-all(bf16[16,5,1152]{2,1,0:T(8,128)(2,1)S(1)} %all_to_all.16), channel_id=1, replica_groups=mesh['ep'=16,'tp'=2] {'ep'}, dimensions={0} | all-to-all | bytes 368640 | tf_op jit(solution)/shard_map/all_to_all | solution.py:129
  76.6 2.1 %all_gather.11 = bf16[80,2304]{1,0:T(8,128)(2,1)S(1)} all-gather(bf16[80,1152]{1,0:T(8,128)(2,1)S(1)} %all_to_all.18), channel_id=1, replica_groups=mesh['ep'=16,'tp'=2] {'tp'}, dimensions={1}, use_global_device_ids=true | all-gather | bytes 552960 | tf_op jit(solution)/shard_map/all_gather | solution.py:130
  78.7 2.2 %fusion.6 = f32[80,512]{1,0:T(8,128)S(1)} fusion(bf16[80,2304]{1,0:T(8,128)(2,1)S(1)} %all_gather.11, bf16[1,2304,512]{2,1,0:T(8,128)(2,1)} %param.32), kind=kOutput, calls=%fused_computation.9 | convolution fusion | flops 188743680 | bytes 2891776 | tf_op jit(solution)/shard_map/dot_general | solution.py:131
  80.8 2.6 %convolution_convert_fusion = bf16[80,2304]{1,0:T(8,128)(2,1)S(1)} fusion(bf16[1,512,2304]{2,1,0:T(8,128)(2,1)S(1)} %copy-done, bf16[80,2304]{1,0:T(8,128)(2,1)S(1)} %all_gather.11, bf16[1,2304,512]{2,1,0:T(8,128)(2,1)} %param.33, f32[80,512]{1,0:T(8,128)S(1)} %fusion.6), kind=kOutput, calls=%fused_computation.2 | convolution fusion | flops 377917440 | bytes 5619712 | tf_op jit(solution)/shard_map/dot_general | solution.py:134
  83.5 1.1 copy.50
  84.6 2.1 %fusion.71 = f32[7,512]{1,0:T(8,128)S(1)} fusion(bf16[7,2304]{1,0:T(8,128)(2,1)S(1)} %fusion.36, bf16[2304,512]{1,0:T(8,128)(2,1)} %param.35), kind=kOutput, calls=%fused_computation.103 | convolution fusion | flops 16515072 | bytes 2405888 | tf_op jit(solution)/shard_map/dot_general | solution.py:99
  86.6 3.9 %reduce-scatter.7.cloned.1.call-done = bf16[1152,80]{1,0:T(8,128)(2,1)} async-done(((bf16[2304,80]{1,0:T(8,128)(2,1)}), bf16[1152,80]{1,0:T(8,128)(2,1)}) %reduce-scatter.7.cloned.1.call-update) | async-done | bytes 184336
  90.5 1.1 copy.51
  91.6 0.8 all_to_all.19
  92.4 6.7 %all-to-all-start.1 = ((bf16[16,5,1152]{2,1,0:T(8,128)(2,1)}), bf16[16,5,1152]{2,1,0:T(8,128)(2,1)S(1)}, u32[]{:S(2)}, u32[]{:S(2)}) async-start(bf16[16,5,1152]{2,1,0:T(8,128)(2,1)} %all_to_all.19), calls=%async_computation.1 | async-start | bytes 589824 | tf_op jit(solution)/shard_map/all_to_all | solution.py:143
  99.2 3.2 %convolution_convert_fusion.1 = bf16[7,2304]{1,0:T(8,128)(2,1)S(1)} fusion(bf16[512,2304]{1,0:T(8,128)(2,1)} %param.37, bf16[7,2304]{1,0:T(8,128)(2,1)S(1)} %fusion.36, bf16[2304,512]{1,0:T(8,128)(2,1)} %param.36, f32[7,512]{1,0:T(8,128)S(1)} %fusion.71), kind=kOutput, calls=%fused_computation.3 | convolution fusion | flops 33067776 | bytes 4797440 | tf_op jit(solution)/shard_map/dot_general | solution.py:102
  102.4 1.1 copy.52
  103.8 9.2 %reduce-scatter.9.cloned.1.call-done = bf16[1152,7]{1,0:T(8,128)(2,1)} async-done(((bf16[2304,7]{1,0:T(8,128)(2,1)}), bf16[1152,7]{1,0:T(8,128)(2,1)}) %reduce-scatter.9.cloned.1.call-update) | async-done | bytes 16144
  113.0 1.1 copy.53
  (70 shorter events, 4.5 us)
Async XLA Ops:
  6.5 74.3 %copy-start = (bf16[1,512,2304]{2,1,0:T(8,128)(2,1)S(1)}, bf16[1,512,2304]{2,1,0:T(8,128)(2,1)}, u32[]{:S(2)}) copy-start(bf16[1,512,2304]{2,1,0:T(8,128)(2,1)} %param.34) | copy-start | bytes 7077892
  6.5 84.0 %reduce-scatter.7.cloned.1.call-start = ((), (), s32[]{:S(2)}) async-start(), calls=%async_computation.4 | async-start | bytes 884736
  11.6 20.6 %copy-start.6 = (s32[7]{0:T(128)S(1)}, s32[7]{0:T(128)}, u32[]{:S(2)}) copy-start(s32[7]{0:T(128)} %param.30) | copy-start | bytes 88
  11.6 20.7 %copy-start.1 = (bf16[7,2304]{1,0:T(8,128)(2,1)S(1)}, bf16[7,2304]{1,0:T(8,128)(2,1)}, u32[]{:S(2)}) copy-start(bf16[7,2304]{1,0:T(8,128)(2,1)} %param.20) | copy-start | bytes 96772
  32.3 11.9 %slice-start = ((s8[4718592]{0:T(1024)(128)(4,1)}), s8[524288]{0:T(1024)(128)(4,1)S(1)}, s32[]{:S(2)}) async-start(s8[4718592]{0:T(1024)(128)(4,1)} %bitcast.90), calls=%async_computation.6 | async-start | bytes 1048576
  35.8 8.2 %copy-start.5 = (f32[8]{0:T(128)S(1)}, f32[8]{0:T(128)}, u32[]{:S(2)}) copy-start(f32[8]{0:T(128)} %param.26) | copy-start | bytes 100
  35.8 8.3 %slice-start.1 = ((s8[4718592]{0:T(1024)(128)(4,1)}), s8[4194304]{0:T(1024)(128)(4,1)S(1)}, s32[]{:S(2)}) async-start(s8[4718592]{0:T(1024)(128)(4,1)} %bitcast.90), calls=%async_computation.7 | async-start | bytes 8388608
  44.2 8.7 %slice-start.2 = ((s8[4718592]{0:T(1024)(128)(4,1)}), s8[4194304]{0:T(1024)(128)(4,1)S(1)}, s32[]{:S(2)}) async-start(s8[4718592]{0:T(1024)(128)(4,1)} %bitcast.92), calls=%async_computation.8 | async-start | bytes 8388608
  44.9 7.8 %copy-start.7 = (bf16[128]{0:T(256)(128)(2,1)S(1)}, bf16[128]{0:T(256)(128)(2,1)}, u32[]{:S(2)}) copy-start(bf16[128]{0:T(256)(128)(2,1)} %param.27) | copy-start | bytes 772
  44.9 7.9 %slice-start.3 = ((s8[4718592]{0:T(1024)(128)(4,1)}), s8[524288]{0:T(1024)(128)(4,1)S(1)}, s32[]{:S(2)}) async-start(s8[4718592]{0:T(1024)(128)(4,1)} %bitcast.92), calls=%async_computation.9 | async-start | bytes 1048576
  52.6 3.8 %copy-start.3 = (bf16[2304]{0:T(1024)(128)(2,1)S(1)}, bf16[2304]{0:T(1024)(128)(2,1)}, u32[]{:S(2)}) copy-start(bf16[2304]{0:T(1024)(128)(2,1)} %param.31) | copy-start | bytes 13828
  52.6 3.8 %copy-start.2 = (s32[7,6]{1,0:T(8,128)S(1)}, s32[7,6]{1,0:T(8,128)}, u32[]{:S(2)}) copy-start(s32[7,6]{1,0:T(8,128)} %param.38) | copy-start | bytes 508
  84.6 19.2 %copy-start.4 = (f32[7,6]{1,0:T(8,128)S(1)}, f32[7,6]{1,0:T(8,128)}, u32[]{:S(2)}) copy-start(f32[7,6]{1,0:T(8,128)} %param.39) | copy-start | bytes 508
  92.4 21.7 %all-to-all-start.1 = ((bf16[16,5,1152]{2,1,0:T(8,128)(2,1)}), bf16[16,5,1152]{2,1,0:T(8,128)(2,1)S(1)}, u32[]{:S(2)}, u32[]{:S(2)}) async-start(bf16[16,5,1152]{2,1,0:T(8,128)(2,1)} %all_to_all.19), calls=%async_computation.1 | async-start | bytes 589824 | tf_op jit(solution)/shard_map/all_to_all | solution.py:143
  99.2 13.8 %reduce-scatter.9.cloned.1.call-start = ((), (), s32[]{:S(2)}) async-start(), calls=%async_computation.5 | async-start | bytes 884736
Sparse Core Ops, SparseCore 0:
  84.7 5.7 reduce-scatter.6
  103.7 9.2 reduce-scatter.8
